TPU v7x, 32 devices: a whole 2x2x4 slice. The times are simulated.
32 devices in a mesh: ep: 8 (over z, x), tp: 4 (over y, core).
Axes of the slice: x: 2, y: 2, z: 4, core: 2. Of those that a mesh axis runs over, the one named last changes fastest.
Arguments:
- mixer_input_rows: bfloat16 [1024, 2048], P('ep'), may hold values from -6 to 6
- mix_gain: float32 [2048], replicated, may hold values from 0.1 to 1.9
- w_recept: bfloat16 [2048, 1024], P(None, 'tp'), may hold values from -0.125 to 0.125
- w_key: bfloat16 [2048, 1024], P(None, 'tp'), may hold values from -0.125 to 0.125
- w_value: bfloat16 [2048, 1024], P(None, 'tp'), may hold values from -0.125 to 0.125
- lowered_map_factor: bfloat16 [2048, 64], replicated, may hold values from -0.125 to 0.125
- decay_up: bfloat16 [64, 1024], P(None, 'tp'), may hold values from -0.75 to 0.75
- rate_up: bfloat16 [64, 1024], P(None, 'tp'), may hold values from -0.75 to 0.75
- decay_base: float32 [1024], P('tp'), may hold values from -13 to -2
- rate_base: float32 [1024], P('tp'), may hold values from -9 to 1
- decay_shift: float32 [1024, 16], P('ep', 'tp'), may hold values from -0.7 to 0, as said below
- out_gain: float32 [1024], P('tp'), may hold values from 0.1 to 1.9
- w_output: bfloat16 [1024, 2048], P('tp'), may hold values from -0.1875 to 0.1875
- moe_rows: bfloat16 [1024, 2048], P('ep'), may hold values from -6 to 6
- moe_gain: float32 [2048], replicated, may hold values from 0.1 to 1.9
- routes: int32 [1024, 2], P('ep'), may hold values from 0 to 7, all different within a row; in each aligned block of 128 rows (0 to 127, 128 to 255, ...) at most 64 rows name the same one
- route_weight: float32 [1024, 2], P('ep'), may hold values from 0.1 to 1
- exp_gate: bfloat16 [8, 2048, 4096], P('ep', None, 'tp'), may hold values from -0.125 to 0.125
- exp_up: bfloat16 [8, 2048, 4096], P('ep', None, 'tp'), may hold values from -0.125 to 0.125
- exp_down: bfloat16 [8, 4096, 2048], P('ep', 'tp'), may hold values from -0.125 to 0.125
Outputs:
- mix_out: bfloat16 [1024, 2048], P(('ep', 'tp'))
- moe_out: bfloat16 [1024, 2048], P('ep', 'tp')
Inputs may be any that keep to these rules, and one draw needn't show every extreme that they name: `routes`: in each aligned block of 128 rows no expert is named more than 64 times, and in some block one expert is named exactly 64 times; the two entries of a row differ. `decay_shift`: at most zero.
All inputs are finite; a program needn't handle non-finite values.
Results may differ from a plain program's by a relative error of at most 0.02.
Values may be sent and summed in bfloat16 or wider, within the bound.
A program may use at most 64 MiB of HBM per device.

v0:
```python
import functools
import math

import jax
import jax.numpy as jnp
from jax import lax
from jax.experimental import pallas as pl
from jax.experimental.pallas import tpu as pltpu
from jax.sharding import PartitionSpec as P

HIGHEST = lax.Precision.HIGHEST
DECAY_SCALE = math.exp(-0.5)


def row_norm(row_block, gain_vector):
    entries = row_block.astype(jnp.float32)
    factor = lax.rsqrt(jnp.mean(entries * entries, axis=-1, keepdims=True) + 1e-06)
    return (entries * factor * gain_vector).astype(jnp.bfloat16)


F32 = jnp.float32
BF16 = jnp.bfloat16
CHUNK = 64


def mul(left, right, left_dim=1, right_dim=0):
    return lax.dot_general(
        left.astype(BF16),
        right.astype(BF16),
        (((left_dim,), (right_dim,)), ((), ())),
        preferred_element_type=F32,
    )


def local_kernel(
    heads,
    width,
    rows_ref,
    gain_ref,
    recept_ref,
    key_ref,
    value_ref,
    low_ref,
    decay_up_ref,
    rate_up_ref,
    decay_base_ref,
    rate_base_ref,
    shift_ref,
    totals_ref,
    read_ref,
    own_ref,
):
    tokens = rows_ref.shape[0]
    chunk = min(CHUNK, tokens)
    chunks = tokens // chunk
    normed = row_norm(rows_ref[...], gain_ref[...])
    recept = jnp.dot(normed, recept_ref[...], preferred_element_type=F32).astype(BF16)
    keys = jnp.dot(normed, key_ref[...], preferred_element_type=F32).astype(BF16).astype(F32)
    values = jnp.dot(normed, value_ref[...], preferred_element_type=F32).astype(BF16)
    recept = recept.astype(F32)
    low = jnp.tanh(jnp.dot(normed, low_ref[...], preferred_element_type=F32)).astype(BF16)
    decay_pre = decay_base_ref[...] + jnp.dot(low, decay_up_ref[...], preferred_element_type=F32)
    rate = jax.nn.sigmoid(
        rate_base_ref[...] + jnp.dot(low, rate_up_ref[...], preferred_element_type=F32)
    )
    shift = shift_ref[...]
    shift_wide = jnp.concatenate(
        [jnp.broadcast_to(shift[:, h : h + 1], (tokens, width)) for h in range(heads)], axis=1
    )
    log_decay = -DECAY_SCALE * jax.nn.sigmoid(decay_pre) + shift_wide

    row = lax.broadcasted_iota(jnp.int32, (tokens, tokens), 0)
    col = lax.broadcasted_iota(jnp.int32, (tokens, tokens), 1)
    same = (row // chunk) == (col // chunk)
    lower = jnp.where(same & (row >= col), 1.0, 0.0).astype(F32)
    running = jnp.dot(lower, log_decay, precision=HIGHEST, preferred_element_type=F32)
    ends = [running[(c + 1) * chunk - 1 : (c + 1) * chunk, :] for c in range(chunks)]
    total = jnp.concatenate(
        [jnp.broadcast_to(end, (chunk, end.shape[1])) for end in ends], axis=0
    )
    half = 0.5 * total
    squares = keys * keys
    unit = jnp.concatenate(
        [
            keys[:, h * width : (h + 1) * width]
            * lax.rsqrt(
                jnp.sum(squares[:, h * width : (h + 1) * width], axis=-1, keepdims=True) + 1e-06
            )
            for h in range(heads)
        ],
        axis=1,
    )
    learned = unit * rate
    sides = []
    for reverse in (False, True):
        upto = total - running + log_decay if reverse else running
        before = upto - log_decay
        up_scale = jnp.exp(upto - half)
        down_scale = jnp.exp(half - upto)
        tail = jnp.exp(total - upto)
        sides.append(
            (
                (unit * jnp.exp(before - half)).astype(BF16),
                (recept * up_scale).astype(BF16),
                (learned * down_scale).astype(BF16),
                (keys * down_scale).astype(BF16),
                unit * jnp.exp(before),
                recept * jnp.exp(upto),
                (learned * tail).astype(BF16),
                (keys * tail).astype(BF16),
            )
        )
    problems = [(h, d) for h in range(heads) for d in range(2)]
    products, inverses, lowers = {}, {}, {}
    for p in problems:
        h, d = p
        cut = slice(h * width, (h + 1) * width)
        a_side, q_side, b_side, c_side = [side[:, cut] for side in sides[d][:4]]
        pair = mul(
            jnp.concatenate([a_side, q_side], axis=0),
            jnp.concatenate([b_side, c_side], axis=0),
            1,
            1,
        )
        strict = same & ((row < col) if d else (row > col))
        whole = same & ((row <= col) if d else (row >= col))
        a_b = jnp.where(strict, pair[:tokens, :tokens], 0.0)
        a_c = jnp.where(strict, pair[:tokens, tokens:], 0.0)
        q_b = jnp.where(whole, pair[tokens:, :tokens], 0.0)
        q_c = jnp.where(whole, pair[tokens:, tokens:], 0.0)
        by_value = mul(jnp.concatenate([a_c, q_c], axis=0), values[:, cut])
        products[p] = (by_value[:tokens], by_value[tokens:], q_b)
        lowers[p] = a_b.astype(BF16)
        near = (row // 2) == (col // 2)
        inverses[p] = jnp.where(row == col, 1.0, jnp.where(near, -a_b, 0.0))
    size = 2
    while size < chunk:
        ring = ((row // (2 * size)) == (col // (2 * size))) & ((row // size) != (col // size))
        right = {
            p: mul(jnp.where(ring, lowers[p], jnp.zeros((), BF16)), inverses[p]) for p in problems
        }
        for p in problems:
            inverses[p] = inverses[p] - mul(inverses[p], right[p])
        size = 2 * size
    eye = lax.broadcasted_iota(jnp.int32, (width, width), 0) == lax.broadcasted_iota(
        jnp.int32, (width, width), 1
    )
    for h in range(heads):
        cut = slice(h * width, (h + 1) * width)
        own_sum = None
        reads = []
        for d in range(2):
            p = (h, d)
            written, read_own, q_b = products[p]
            a_full, q_full, b_tail, c_tail = [side[:, cut] for side in sides[d][4:]]
            solved = mul(inverses[p], jnp.concatenate([written, a_full], axis=1))
            back = mul(q_b, solved)
            own = read_own - back[:, :width]
            gain = q_full - back[:, width:]
            order = range(chunks - 1, -1, -1) if d else range(chunks)
            carry = None
            owns, gains = [None] * chunks, [None] * chunks
            for c in order:
                part = slice(c * chunk, (c + 1) * chunk)
                joint = mul(solved[part], b_tail[part], 0, 0)
                decayed = jnp.exp(ends[c][:, cut])
                step_p = jnp.where(eye, decayed, 0.0) - joint[width:]
                step_q = mul(values[part, cut], c_tail[part], 0, 0) - joint[:width]
                if carry is None:
                    owns[c], gains[c] = own[part], gain[part]
                    carry = jnp.concatenate([step_p, step_q], axis=0)
                else:
                    moved = mul(gain[part], carry, 1, 1)
                    gains[c] = moved[:, :width]
                    owns[c] = own[part] + moved[:, width:]
                    carry = mul(carry, step_p)
                    carry = jnp.concatenate([carry[:width], carry[width:] + step_q], axis=0)
            totals_ref[d, h] = jnp.concatenate([carry[:width], carry[width:]], axis=1).astype(BF16)
            reads.append(jnp.concatenate(gains, axis=0))
            own_whole = jnp.concatenate(owns, axis=0)
            own_sum = own_whole if own_sum is None else own_sum + own_whole
        read_ref[:, 2 * h * width : 2 * (h + 1) * width] = jnp.concatenate(reads, axis=1).astype(
            BF16
        )
        own_ref[:, cut] = own_sum


def finish_kernel(heads, width, where_ref, totals_ref, read_ref, own_ref, gain_ref, out_ref, res):
    me = where_ref[0]
    count = totals_ref.shape[0]
    states = {(d, h): jnp.zeros((width, width), F32) for d in range(2) for h in range(heads)}
    for j in range(count):
        for d in range(2):
            owner = count - 1 - j if d else j
            active = (owner > me) if d else (owner < me)
            for h in range(heads):
                both = totals_ref[owner, d, h]
                fresh = mul(states[d, h], both[:, :width]) + both[:, width:].astype(F32)
                states[d, h] = jnp.where(active, fresh, states[d, h])
    parts = []
    for h in range(heads):
        cut = slice(h * width, (h + 1) * width)
        pair = jnp.concatenate([states[0, h], states[1, h]], axis=1)
        mixed = own_ref[:, cut] + mul(
            read_ref[:, 2 * h * width : 2 * (h + 1) * width], pair, 1, 1
        )
        centre = mixed - jnp.mean(mixed, axis=-1, keepdims=True)
        parts.append(
            centre * lax.rsqrt(jnp.mean(centre * centre, axis=-1, keepdims=True) + 1e-05)
        )
    grouped = (jnp.concatenate(parts, axis=1) * gain_ref[...]).astype(BF16)
    res[...] = jnp.dot(grouped, out_ref[...], preferred_element_type=F32).astype(BF16)


def local_pass(heads, width, *operands):
    tokens = operands[0].shape[0]
    return pl.pallas_call(
        functools.partial(local_kernel, heads, width),
        out_shape=(
            jax.ShapeDtypeStruct((2, heads, width, 2 * width), BF16),
            jax.ShapeDtypeStruct((tokens, 2 * heads * width), BF16),
            jax.ShapeDtypeStruct((tokens, heads * width), F32),
        ),
        in_specs=[pl.BlockSpec(memory_space=pltpu.VMEM)] * len(operands),
        out_specs=(pl.BlockSpec(memory_space=pltpu.VMEM),) * 3,
        cost_estimate=pl.CostEstimate(
            flops=2000000000, bytes_accessed=20000000, transcendentals=0
        ),
        name="mix_local",
    )(*operands)


def finish_pass(heads, width, where, totals, read, own, gain, w_output):
    return pl.pallas_call(
        functools.partial(finish_kernel, heads, width),
        out_shape=jax.ShapeDtypeStruct((own.shape[0], w_output.shape[1]), BF16),
        in_specs=[pl.BlockSpec(memory_space=pltpu.SMEM)]
        + [pl.BlockSpec(memory_space=pltpu.VMEM)] * 5,
        out_specs=pl.BlockSpec(memory_space=pltpu.VMEM),
        cost_estimate=pl.CostEstimate(
            flops=1000000000, bytes_accessed=10000000, transcendentals=0
        ),
        name="mix_finish",
    )(where, totals, read, own, gain, w_output)


def route_tables(route_rows, weight_rows, expert_count, slot_count):
    route_list = route_rows.reshape(-1)
    onehot = (route_list[:, None] == jnp.arange(expert_count, dtype=jnp.int32)[None, :]).astype(
        jnp.int32
    )
    slot_index = jnp.sum((jnp.cumsum(onehot, axis=0) - onehot) * onehot, axis=1)
    target = (route_list * slot_count + slot_index).reshape(route_rows.shape)
    columns = jnp.arange(expert_count * slot_count, dtype=jnp.int32)
    matches = target[:, :, None] == columns[None, None, :]
    placing = jnp.sum(matches.astype(jnp.int32), axis=1).astype(jnp.bfloat16)
    rounded = weight_rows.astype(jnp.bfloat16)
    weighing = jnp.sum(jnp.where(matches, rounded[:, :, None], jnp.zeros((), jnp.bfloat16)), axis=1)
    return (placing, weighing)


def expert_hidden(slot_rows, gate_shard, up_shard):
    flattened = slot_rows.reshape(-1, slot_rows.shape[-1])
    gate_part = jnp.dot(flattened, gate_shard, preferred_element_type=jnp.float32)
    up_part = jnp.dot(flattened, up_shard, preferred_element_type=jnp.float32)
    hidden = (jax.nn.silu(gate_part) * up_part).astype(jnp.bfloat16)
    return hidden.reshape(slot_rows.shape[:-1] + (gate_shard.shape[1],))


def shards(
    mixer_input_rows,
    mix_gain,
    w_recept,
    w_key,
    w_value,
    lowered_map_factor,
    decay_up,
    rate_up,
    decay_base,
    rate_base,
    decay_shift,
    out_gain,
    w_output,
    moe_rows,
    moe_gain,
    routes,
    route_weight,
    exp_gate,
    exp_up,
    exp_down,
):
    head_count = decay_shift.shape[1]
    head_width = w_recept.shape[1] // head_count
    totals, read, own = local_pass(
        head_count,
        head_width,
        mixer_input_rows,
        mix_gain[None],
        w_recept,
        w_key,
        w_value,
        lowered_map_factor,
        decay_up,
        rate_up,
        decay_base[None],
        rate_base[None],
        decay_shift,
    )
    gathered = lax.all_gather(totals[None], "ep", axis=0, tiled=True)
    where = lax.axis_index("ep").astype(jnp.int32)[None]
    partial_mix = finish_pass(
        head_count, head_width, where, gathered, read, own, out_gain[None], w_output
    )
    mix_out = lax.psum_scatter(partial_mix, "tp", scatter_dimension=0, tiled=True)
    group_rows = moe_rows.shape[0]
    experts = lax.axis_size("ep")
    slots = 4 * group_rows // experts
    moe_normed = row_norm(moe_rows, moe_gain)
    placing, weighing = route_tables(routes, route_weight, experts, slots)
    buffer = lax.dot_general(
        placing, moe_normed, (((0,), (0,)), ((), ())), preferred_element_type=jnp.float32
    )
    buffer = buffer.astype(jnp.bfloat16).reshape(experts, slots, -1)
    gate_shard = exp_gate[0]
    up_shard = exp_up[0]
    down_shard = exp_down[0]
    arrived = lax.all_to_all(buffer, "ep", split_axis=0, concat_axis=0, tiled=True)
    hidden = expert_hidden(arrived, gate_shard, up_shard)
    partial_sum = jnp.dot(
        hidden.reshape(-1, hidden.shape[-1]), down_shard, preferred_element_type=jnp.float32
    )
    partial_sum = partial_sum.reshape(experts, slots, -1)
    summed = lax.psum_scatter(
        partial_sum.astype(jnp.bfloat16), "tp", scatter_dimension=2, tiled=True
    )
    returned = lax.all_to_all(summed, "ep", split_axis=0, concat_axis=0, tiled=True)
    moe_out = jnp.dot(
        weighing, returned.reshape(experts * slots, -1), preferred_element_type=jnp.float32
    )
    return (mix_out, moe_out.astype(jnp.bfloat16))


def solution(mesh):
    return jax.shard_map(
        shards,
        mesh=mesh,
        in_specs=(
            P("ep", None),
            P(),
            P(None, "tp"),
            P(None, "tp"),
            P(None, "tp"),
            P(),
            P(None, "tp"),
            P(None, "tp"),
            P("tp"),
            P("tp"),
            P("ep", "tp"),
            P("tp"),
            P("tp", None),
            P("ep", None),
            P(),
            P("ep", None),
            P("ep", None),
            P("ep", None, "tp"),
            P("ep", None, "tp"),
            P("ep", "tp", None),
        ),
        out_specs=(P(("ep", "tp"), None), P("ep", "tp")),
        check_vma=False,
    )
```

profile of v0, /device:TPU:1, one launch (start us, length us, event | category | flops | bytes accessed | tf_op | source)
XLA Modules:
  0.0 167.6 jit_solution(11515040085093501696)
XLA Ops:
  8.0 0.0 reduce-scatter.5.cloned.1.call-start
  8.0 0.8 copy.49
  8.8 0.1 eq.42
  9.0 0.1 eq.38
  9.1 0.6 reduce-window.6
  9.7 0.2 slice_reduce_fusion
  10.0 0.1 fusion.21
  10.1 0.1 reduce_sum.42
  10.2 0.1 copy.51
  10.3 0.7 multiply_add_fusion
  11.0 0.1 convert_reduce_fusion
  11.1 1.2 fusion.11
  12.3 1.9 %convolution_convert_fusion = bf16[512,2048]{1,0:T(8,128)(2,1)S(1)} fusion(bf16[128,2048]{1,0:T(8,128)(2,1)} %param.33, f32[2048]{0:T(1024)} %param.34, f32[128]{0:T(128)S(1)} %add_rsqrt_fusion, s32[128,512]{1,0:T(8,128)S(1)} %convert_reduce_fusion), kind=kOutput, calls=%fused_computation.7 | convolution fusion | flops 270598144 | bytes 2892288 | tf_op jit(solution)/shard_map/dot_general | solution.py:320
  14.2 0.0 copy-start.2
  14.2 53.7 %all_to_all.10 = bf16[8,64,2048]{2,1,0:T(8,128)(2,1)S(1)} all-to-all(bf16[8,64,2048]{2,1,0:T(8,128)(2,1)S(1)} %bitcast.37), channel_id=1, replica_groups=mesh['ep'=8,'tp'=4] {'ep'}, dimensions={0} | all-to-all | bytes 4194304 | tf_op jit(solution)/shard_map/all_to_all | solution.py:327
  67.9 0.0 copy-done.2
  67.9 0.0 copy-start.3
  68.0 2.3 %fusion.4 = f32[512,1024]{1,0:T(8,128)S(1)} fusion(bf16[512,2048]{1,0:T(8,128)(2,1)S(1)} %bitcast.38, bf16[1,2048,1024]{2,1,0:T(8,128)(2,1)S(1)} %copy-done.2), kind=kOutput, calls=%fused_computation.4 | convolution fusion | flops 2147483648 | bytes 8388608 | tf_op jit(solution)/shard_map/dot_general | solution.py:264
  70.3 0.0 copy-done.3
  70.3 0.0 copy-start.4
  70.3 2.5 %multiply_convert_fusion = bf16[512,1024]{1,0:T(8,128)(2,1)S(1)} fusion(f32[512,1024]{1,0:T(8,128)S(1)} %fusion.4, bf16[512,2048]{1,0:T(8,128)(2,1)S(1)} %bitcast.39, bf16[1,2048,1024]{2,1,0:T(8,128)(2,1)S(1)} %copy-done.3), kind=kOutput, calls=%fused_computation.8 | convolution fusion | flops 2150629376 | bytes 9437184 | tf_op jit(solution)/shard_map/dot_general | solution.py:265
  72.8 0.0 copy-done.4
  72.9 3.7 %fusion.6 = bf16[8,64,2048]{2,1,0:T(8,128)(2,1)} fusion(bf16[8,64,1024]{2,1,0:T(8,128)(2,1)S(1)} %bitcast.46, bf16[1,1024,2048]{2,1,0:T(8,128)(2,1)S(1)} %copy-done.4), kind=kOutput, calls=%fused_computation.6 | convolution fusion | flops 2148532224 | bytes 7340032 | tf_op jit(solution)/shard_map/dot_general | solution.py:329
  76.6 0.0 copy-start
  76.6 0.0 copy-start.1
  76.6 0.0 reduce-scatter.5.cloned.1.call-update
  76.6 0.2 all-gather.3.cloned.1.call-start
  76.8 0.7 copy-done
  77.5 1.0 copy.47.low_ref
  78.5 0.0 copy-done.1
  78.5 0.7 copy.48.shift_ref
  79.3 10.1 %mix_local.1 = (bf16[2,4,64,128]{3,2,1,0:T(8,128)(2,1)}, bf16[128,512]{1,0:T(8,128)(2,1)}, f32[128,256]{1,0:T(8,128)}) custom-call(bf16[128,2048]{1,0:T(8,128)(2,1)} %rows_ref.1, f32[1,2048]{1,0:T(1,128)} %bitcast.42, bf16[2048,256]{1,0:T(8,128)(2,1)} %recept_ref.1, bf16[2048,256]{1,0:T(8,128)(2,1)} %key_ref.1, bf16[2048,256]{1,0:T(8,128)(2,1)} %value_ref.1, ...), custom_call_target="tpu_custom_call" | custom-call | flops 2000000000 | bytes 20000000 | tf_op jit(solution)/shard_map/mix_local/pallas_call | solution.py:217
  89.3 0.0 all-gather.3.cloned.1.call-update
  89.4 18.6 %reduce-scatter.5.cloned.1.call-done = bf16[8,64,512]{2,1,0:T(8,128)(2,1)} async-done(((bf16[8,64,2048]{2,1,0:T(8,128)(2,1)}), bf16[8,64,512]{2,1,0:T(8,128)(2,1)}) %reduce-scatter.5.cloned.1.call-update) | async-done | bytes 524304 | tf_op jit(solution)/shard_map/reduce_scatter | solution.py:333
  108.0 5.2 %all-to-all-start.1 = ((bf16[8,64,512]{2,1,0:T(8,128)(2,1)}), bf16[8,64,512]{2,1,0:T(8,128)(2,1)S(1)}, u32[]{:S(2)}, u32[]{:S(2)}) async-start(bf16[8,64,512]{2,1,0:T(8,128)(2,1)} %reduce-scatter.5.cloned.1.call-done), calls=%async_computation.3 | async-start | bytes 1048576 | tf_op jit(solution)/shard_map/all_to_all | solution.py:336
  113.2 0.0 reduce-scatter.3.cloned.1.call-start
  113.2 22.8 %all-gather.3.cloned.1.call-done = bf16[16,4,64,128]{3,2,1,0:T(8,128)(2,1)} async-done(((bf16[2,4,64,128]{3,2,1,0:T(8,128)(2,1)}), bf16[16,4,64,128]{3,2,1,0:T(8,128)(2,1)}) %all-gather.3.cloned.1.call-update) | async-done | bytes 1048592 | tf_op jit(solution)/shard_map/all_gather | solution.py:309
  136.0 0.0 copy-start.5
  136.0 4.8 %mix_finish.1 = bf16[128,2048]{1,0:T(8,128)(2,1)} custom-call(s32[1]{0:T(128)} %bitcast.where_ref, bf16[8,2,4,64,128]{4,3,2,1,0:T(8,128)(2,1)} %bitcast.41, bf16[128,512]{1,0:T(8,128)(2,1)} %get-tuple-element.6.read_ref, f32[128,256]{1,0:T(8,128)} %get-tuple-element.7.own_ref, f32[1,256]{1,0:T(1,128)} %bitcast.45, bf16[256,2048]{1,0:T(8,128)(2,1)} %out_ref.1), custom_call_target="tpu_custom_call" | custom-call | flops 1000000000 | bytes 10000000 | tf_op jit(solution)/shard_map/mix_finish/pallas_call | solution.py:234
  140.8 0.0 reduce-scatter.3.cloned.1.call-update
  140.8 0.0 copy-done.5
  140.9 0.1 fusion.18
  141.0 0.0 all-to-all-done.1
  141.0 0.9 convolution_convert_fusion.1
  141.9 18.2 %reduce-scatter.3.cloned.1.call-done = bf16[32,2048]{1,0:T(8,128)(2,1)} async-done(((bf16[128,2048]{1,0:T(8,128)(2,1)}), bf16[32,2048]{1,0:T(8,128)(2,1)}) %reduce-scatter.3.cloned.1.call-update) | async-done | bytes 131088 | tf_op jit(solution)/shard_map/reduce_scatter | solution.py:314
  (5 shorter events, 0.1 us)
Async XLA Ops:
  8.0 100.0 %reduce-scatter.5.cloned.1.call-start = ((), (), s32[]{:S(2)}) async-start(), calls=%async_computation.5 | async-start | bytes 2621440 | tf_op jit(solution)/shard_map/reduce_scatter | solution.py:333
  14.2 53.8 %copy-start.2 = (bf16[1,2048,1024]{2,1,0:T(8,128)(2,1)S(1)}, bf16[1,2048,1024]{2,1,0:T(8,128)(2,1)}, u32[]{:S(2)}) copy-start(bf16[1,2048,1024]{2,1,0:T(8,128)(2,1)} %param.37) | copy-start | bytes 12582916
  67.9 2.4 %copy-start.3 = (bf16[1,2048,1024]{2,1,0:T(8,128)(2,1)S(1)}, bf16[1,2048,1024]{2,1,0:T(8,128)(2,1)}, u32[]{:S(2)}) copy-start(bf16[1,2048,1024]{2,1,0:T(8,128)(2,1)} %param.38) | copy-start | bytes 12582916
  70.3 2.5 %copy-start.4 = (bf16[1,1024,2048]{2,1,0:T(8,128)(2,1)S(1)}, bf16[1,1024,2048]{2,1,0:T(8,128)(2,1)}, u32[]{:S(2)}) copy-start(bf16[1,1024,2048]{2,1,0:T(8,128)(2,1)} %param.39) | copy-start | bytes 12582916
  76.6 0.9 copy-start
  76.6 2.0 %copy-start.1 = (f32[128,4]{0,1:T(4,128)S(1)}, f32[128,4]{0,1:T(4,128)}, u32[]{:S(2)}) copy-start(f32[128,4]{0,1:T(4,128)} %param.30) | copy-start | bytes 6148
  76.6 59.4 %all-gather.3.cloned.1.call-start = ((), (), s32[]{:S(2)}) async-start(), calls=%async_computation.6 | async-start | bytes 1179648 | tf_op jit(solution)/shard_map/all_gather | solution.py:309
  108.0 33.1 %all-to-all-start.1 = ((bf16[8,64,512]{2,1,0:T(8,128)(2,1)}), bf16[8,64,512]{2,1,0:T(8,128)(2,1)S(1)}, u32[]{:S(2)}, u32[]{:S(2)}) async-start(bf16[8,64,512]{2,1,0:T(8,128)(2,1)} %reduce-scatter.5.cloned.1.call-done), calls=%async_computation.3 | async-start | bytes 1048576 | tf_op jit(solution)/shard_map/all_to_all | solution.py:336
  113.2 47.0 %reduce-scatter.3.cloned.1.call-start = ((), (), s32[]{:S(2)}) async-start(), calls=%async_computation.4 | async-start | bytes 655360 | tf_op jit(solution)/shard_map/reduce_scatter | solution.py:314
  136.0 4.8 %copy-start.5 = (f32[128,2]{0,1:T(2,128)S(1)}, f32[128,2]{0,1:T(2,128)}, u32[]{:S(2)}) copy-start(f32[128,2]{0,1:T(2,128)} %param.36) | copy-start | bytes 3076
Sparse Core Ops, SparseCore 0:
  76.7 31.1 reduce-scatter.4
  141.0 19.1 reduce-scatter.2
Sparse Core Ops, SparseCore 1:
  89.5 46.5 all-gather.2
where the time goes:
time: 169 us; the launch traced here: 168 us
  waiting for transfers between devices  59.7 us (35%)
  blocking collectives  53.7 us (32%)
  between operations  15.6 us (9%)
  Pallas kernels  14.9 us (9%)
  matrix products  11.3 us (7%)
  starting transfers between devices  5.53 us (3%)
  local copies, waits for them, and re-layouts  3.93 us (2%)
  other arithmetic  2.92 us (2%)
    all_to_all x1, blocking collectives, shards(): lax.all_to_all(buffer, 'ep', split_axis=0, concat_axis=0, tiled=True)  53.7 us
    all_gather x1, waiting for transfers between devices, shards(): gathered = lax.all_gather(totals[None], 'ep', axis=0, tiled=True)  22.8 us
    reduce_scatter x1, waiting for transfers between devices, shards(): lax.psum_scatter(partial_sum.astype(jnp.bfloat16), 'tp', scatter_dimensio...  18.6 us
    reduce_scatter x1, waiting for transfers between devices, shards(): lax.psum_scatter(partial_mix, 'tp', scatter_dimension=0, tiled=True)  18.2 us
    pallas_call x1, Pallas kernels, local_pass(): pl.pallas_call(functools.partial(local_kernel, heads, width), out_shape=(...  10.1 us
    all_to_all x1, starting transfers between devices, shards(): lax.all_to_all(summed, 'ep', split_axis=0, concat_axis=0, tiled=True)  5.23 us
    pallas_call x1, Pallas kernels, finish_pass(): pl.pallas_call(functools.partial(finish_kernel, heads, width), out_shape=...  4.79 us
    dot_general x1, matrix products, shards(): jnp.dot(hidden.reshape(-1, hidden.shape[-1]), down_shard, preferred_eleme...  3.72 us
  transfers between devices with their start and end apart: 4, of which 3 were waited for; matrix products, arithmetic and copies ran while one was open for 2% of the time, Pallas kernels for 9%

commit v1 on v0

--- a/solution.py
+++ b/solution.py
@@ -194,7 +194,7 @@
             owner = count - 1 - j if d else j
             active = (owner > me) if d else (owner < me)
             for h in range(heads):
-                both = totals_ref[owner, d, h]
+                both = totals_ref[owner, h]
                 fresh = mul(states[d, h], both[:, :width]) + both[:, width:].astype(F32)
                 states[d, h] = jnp.where(active, fresh, states[d, h])
     parts = []
@@ -242,6 +242,286 @@
         ),
         name="mix_finish",
     )(where, totals, read, own, gain, w_output)
+
+
+MESH_ID = pl.DeviceIdType.MESH
+
+
+def greet(ep_count, tp_count):
+    me, lane = lax.axis_index("ep"), lax.axis_index("tp")
+    barrier = pltpu.get_barrier_semaphore()
+    for k in range(1, ep_count):
+        pl.semaphore_signal(
+            barrier, inc=1, device_id=(lax.rem(me + k, ep_count), lane), device_id_type=MESH_ID
+        )
+    for k in range(1, tp_count):
+        pl.semaphore_signal(
+            barrier, inc=1, device_id=(me, lax.rem(lane + k, tp_count)), device_id_type=MESH_ID
+        )
+    pl.semaphore_wait(barrier, ep_count + tp_count - 2)
+
+
+def remote(source, target, send_sem, recv_sem, device):
+    return pltpu.make_async_remote_copy(
+        src_ref=source,
+        dst_ref=target,
+        send_sem=send_sem,
+        recv_sem=recv_sem,
+        device_id=device,
+        device_id_type=MESH_ID,
+    )
+
+
+def dispatch_kernel(
+    ep_count,
+    tp_count,
+    buffer_ref,
+    totals_ref,
+    arrived_ref,
+    gathered_ref,
+    ep_send,
+    ep_recv,
+    row_send,
+    row_recv,
+    pair_send,
+    pair_recv,
+    total_send,
+    total_recv,
+    keep_sem,
+):
+    me, lane = lax.axis_index("ep"), lax.axis_index("tp")
+    width = buffer_ref.shape[2] // tp_count
+    rows = tp_count // 2
+    mate = lane + 1 - 2 * lax.rem(lane, 2)
+    greet(ep_count, tp_count)
+
+    def columns(of):
+        return pl.ds(pl.multiple_of(of * width, width), width)
+
+    first, second, third, sums = [], [], [], []
+    for k in range(1, ep_count):
+        peer = lax.rem(me + k, ep_count)
+        copy = remote(
+            buffer_ref.at[peer, :, columns(lane)],
+            arrived_ref.at[me, :, columns(lane)],
+            ep_send.at[k],
+            ep_recv.at[k],
+            (peer, lane),
+        )
+        copy.start()
+        first.append(copy)
+    for k in range(1, ep_count):
+        peer = lax.rem(me + k, ep_count)
+        direction = jnp.where(peer > me, 0, 1)
+        copy = remote(
+            totals_ref.at[direction],
+            gathered_ref.at[me],
+            total_send.at[k],
+            total_recv.at[k],
+            (peer, lane),
+        )
+        copy.start()
+        sums.append(copy)
+    keep = pltpu.make_async_copy(buffer_ref.at[me], arrived_ref.at[me], keep_sem.at[0])
+    keep.start()
+    keep_total = pltpu.make_async_copy(totals_ref.at[0], gathered_ref.at[me], keep_sem.at[1])
+    keep_total.start()
+    for k in range(1, ep_count):
+        owner = lax.rem(me + ep_count - k, ep_count)
+        first[k - 1].wait_recv()
+        block = arrived_ref.at[owner, :, columns(lane)]
+        for j in range(1, rows):
+            copy = remote(
+                block,
+                block,
+                row_send.at[j, k],
+                row_recv.at[j, k],
+                (me, lax.rem(lane + 2 * j, tp_count)),
+            )
+            copy.start()
+            second.append((j, owner, k, copy))
+        copy = remote(block, block, pair_send.at[0, k], pair_recv.at[0, k], (me, mate))
+        copy.start()
+        third.append(copy)
+    for j, owner, k, copy in second:
+        copy.wait_recv()
+        block = arrived_ref.at[owner, :, columns(lax.rem(lane + tp_count - 2 * j, tp_count))]
+        passed = remote(block, block, pair_send.at[j, k], pair_recv.at[j, k], (me, mate))
+        passed.start()
+        third.append(passed)
+    for copy in third:
+        copy.wait_recv()
+    for copy in sums:
+        copy.wait_recv()
+    for copy in first + [item[3] for item in second] + third + sums:
+        copy.wait_send()
+    keep.wait()
+    keep_total.wait()
+
+
+def dispatch_pass(ep_count, tp_count, buffer, totals):
+    rows = tp_count // 2
+    dma = pltpu.SemaphoreType.DMA
+    return pl.pallas_call(
+        functools.partial(dispatch_kernel, ep_count, tp_count),
+        out_shape=(
+            jax.ShapeDtypeStruct(buffer.shape, BF16),
+            jax.ShapeDtypeStruct((ep_count,) + totals.shape[1:], BF16),
+        ),
+        in_specs=[pl.BlockSpec(memory_space=pltpu.VMEM)] * 2,
+        out_specs=(pl.BlockSpec(memory_space=pltpu.VMEM),) * 2,
+        scratch_shapes=[
+            dma((ep_count,)),
+            dma((ep_count,)),
+            dma((rows, ep_count)),
+            dma((rows, ep_count)),
+            dma((rows, ep_count)),
+            dma((rows, ep_count)),
+            dma((ep_count,)),
+            dma((ep_count,)),
+            dma((2,)),
+        ],
+        compiler_params=pltpu.CompilerParams(collective_id=1, has_side_effects=True),
+        name="dispatch",
+    )(buffer, totals)
+
+
+def return_kernel(
+    ep_count,
+    tp_count,
+    partial_ref,
+    mix_ref,
+    back_ref,
+    mix_out_ref,
+    pair_in,
+    pair_sum,
+    row_in,
+    result,
+    mix_in,
+    pair_send,
+    pair_recv,
+    row_send,
+    row_recv,
+    ep_send,
+    ep_recv,
+    mix_send,
+    mix_recv,
+):
+    me, lane = lax.axis_index("ep"), lax.axis_index("tp")
+    width = partial_ref.shape[2] // tp_count
+    rows = tp_count // 2
+    core = lax.rem(lane, 2)
+    mine = lane // 2
+    mate = lane + 1 - 2 * core
+    mix_rows = mix_out_ref.shape[0]
+    greet(ep_count, tp_count)
+
+    def columns(of):
+        return pl.ds(pl.multiple_of(of * width, width), width)
+
+    groups = [lax.rem(me + k, ep_count) for k in range(1, ep_count + 1)]
+    first = []
+    for k, group in enumerate(groups):
+        for j in range(rows):
+            copy = remote(
+                partial_ref.at[group, :, columns(2 * j + 1 - core)],
+                pair_in.at[k, j],
+                pair_send.at[k, j],
+                pair_recv.at[k, j],
+                (me, mate),
+            )
+            copy.start()
+            first.append(copy)
+    second = []
+    for k, group in enumerate(groups):
+        for j in range(rows):
+            first[k * rows + j].wait_recv()
+        for j in range(rows):
+            target = lax.rem(mine + j, rows)
+            pair_sum[k, j] = (
+                partial_ref[group, :, columns(2 * target + core)].astype(F32)
+                + pair_in[k, target].astype(F32)
+            ).astype(BF16)
+            if j > 0:
+                copy = remote(
+                    pair_sum.at[k, j],
+                    row_in.at[k, j],
+                    row_send.at[k, j],
+                    row_recv.at[k, j],
+                    (me, 2 * target + core),
+                )
+                copy.start()
+                second.append(copy)
+    mixes = []
+    for j in range(1, tp_count):
+        peer = lax.rem(lane + j, tp_count)
+        copy = remote(
+            mix_ref.at[pl.ds(pl.multiple_of(peer * mix_rows, mix_rows), mix_rows)],
+            mix_in.at[j],
+            mix_send.at[j],
+            mix_recv.at[j],
+            (me, peer),
+        )
+        copy.start()
+        mixes.append(copy)
+    third = []
+    for k, group in enumerate(groups):
+        total = pair_sum[k, 0].astype(F32)
+        for j in range(1, rows):
+            second[k * (rows - 1) + j - 1].wait_recv()
+            total = total + row_in[k, j].astype(F32)
+        if k < ep_count - 1:
+            result[k] = total.astype(BF16)
+            copy = remote(
+                result.at[k], back_ref.at[me], ep_send.at[k], ep_recv.at[k], (group, lane)
+            )
+            copy.start()
+            third.append(copy)
+        else:
+            back_ref[me] = total.astype(BF16)
+    own = mix_ref[pl.ds(pl.multiple_of(lane * mix_rows, mix_rows), mix_rows), :].astype(F32)
+    for j in range(1, tp_count):
+        mixes[j - 1].wait_recv()
+        own = own + mix_in[j].astype(F32)
+    mix_out_ref[...] = own.astype(BF16)
+    for copy in third:
+        copy.wait_recv()
+    for copy in first + second + mixes + third:
+        copy.wait_send()
+
+
+def return_pass(ep_count, tp_count, partial_sum, partial_mix):
+    rows = tp_count // 2
+    dma = pltpu.SemaphoreType.DMA
+    slots, features = partial_sum.shape[1:]
+    width = features // tp_count
+    mix_rows = partial_mix.shape[0] // tp_count
+    return pl.pallas_call(
+        functools.partial(return_kernel, ep_count, tp_count),
+        out_shape=(
+            jax.ShapeDtypeStruct((ep_count, slots, width), BF16),
+            jax.ShapeDtypeStruct((mix_rows, features), BF16),
+        ),
+        in_specs=[pl.BlockSpec(memory_space=pltpu.VMEM)] * 2,
+        out_specs=(pl.BlockSpec(memory_space=pltpu.VMEM),) * 2,
+        scratch_shapes=[
+            pltpu.VMEM((ep_count, rows, slots, width), BF16),
+            pltpu.VMEM((ep_count, rows, slots, width), BF16),
+            pltpu.VMEM((ep_count, rows, slots, width), BF16),
+            pltpu.VMEM((ep_count, slots, width), BF16),
+            pltpu.VMEM((tp_count, mix_rows, features), BF16),
+            dma((ep_count, rows)),
+            dma((ep_count, rows)),
+            dma((ep_count, rows)),
+            dma((ep_count, rows)),
+            dma((ep_count,)),
+            dma((ep_count,)),
+            dma((tp_count,)),
+            dma((tp_count,)),
+        ],
+        compiler_params=pltpu.CompilerParams(collective_id=2, has_side_effects=True),
+        name="return",
+    )(partial_sum, partial_mix)
 
 
 def route_tables(route_rows, weight_rows, expert_count, slot_count):
@@ -306,12 +586,6 @@
         rate_base[None],
         decay_shift,
     )
-    gathered = lax.all_gather(totals[None], "ep", axis=0, tiled=True)
-    where = lax.axis_index("ep").astype(jnp.int32)[None]
-    partial_mix = finish_pass(
-        head_count, head_width, where, gathered, read, own, out_gain[None], w_output
-    )
-    mix_out = lax.psum_scatter(partial_mix, "tp", scatter_dimension=0, tiled=True)
     group_rows = moe_rows.shape[0]
     experts = lax.axis_size("ep")
     slots = 4 * group_rows // experts
@@ -324,16 +598,30 @@
     gate_shard = exp_gate[0]
     up_shard = exp_up[0]
     down_shard = exp_down[0]
-    arrived = lax.all_to_all(buffer, "ep", split_axis=0, concat_axis=0, tiled=True)
+    lanes = lax.axis_size("tp")
+    small = experts <= 8 and lanes == 4
+    if small:
+        arrived, gathered = dispatch_pass(experts, lanes, buffer, totals)
+    else:
+        arrived = lax.all_to_all(buffer, "ep", split_axis=0, concat_axis=0, tiled=True)
+        both = lax.all_gather(totals[None], "ep", axis=0, tiled=True)
+        owners = jnp.arange(experts)[:, None, None, None]
+        gathered = jnp.where(owners < lax.axis_index("ep"), both[:, 0], both[:, 1])
+    where = lax.axis_index("ep").astype(jnp.int32)[None]
+    partial_mix = finish_pass(
+        head_count, head_width, where, gathered, read, own, out_gain[None], w_output
+    )
     hidden = expert_hidden(arrived, gate_shard, up_shard)
     partial_sum = jnp.dot(
         hidden.reshape(-1, hidden.shape[-1]), down_shard, preferred_element_type=jnp.float32
     )
-    partial_sum = partial_sum.reshape(experts, slots, -1)
-    summed = lax.psum_scatter(
-        partial_sum.astype(jnp.bfloat16), "tp", scatter_dimension=2, tiled=True
-    )
-    returned = lax.all_to_all(summed, "ep", split_axis=0, concat_axis=0, tiled=True)
+    partial_sum = partial_sum.reshape(experts, slots, -1).astype(jnp.bfloat16)
+    if small:
+        returned, mix_out = return_pass(experts, lanes, partial_sum, partial_mix)
+    else:
+        mix_out = lax.psum_scatter(partial_mix, "tp", scatter_dimension=0, tiled=True)
+        summed = lax.psum_scatter(partial_sum, "tp", scatter_dimension=2, tiled=True)
+        returned = lax.all_to_all(summed, "ep", split_axis=0, concat_axis=0, tiled=True)
     moe_out = jnp.dot(
         weighing, returned.reshape(experts * slots, -1), preferred_element_type=jnp.float32
     )

time: 169 us -> 102 us (0.60)
  Pallas kernels: 14.9 us -> 75.5 us
  waiting for transfers between devices: 59.7 us -> 0 us
  blocking collectives: 53.7 us -> 0 us
  between operations: 15.6 us -> 0.75 us
  starting transfers between devices: 5.53 us -> 0 us
  matrix products: 11.3 us -> 14.9 us
  local copies, waits for them, and re-layouts: 3.93 us -> 6.43 us
    pallas_call x0 -> x2, Pallas kernels: none -> 60.6 us  [the longest x1 31.7 us: return_pass(): pl.pallas_call(functools.partial(return_kernel, ep_count, tp_count), out_...]
    all_to_all x1 -> x0, blocking collectives: 53.7 us -> none  [shards(): lax.all_to_all(buffer, 'ep', split_axis=0, concat_axis=0, tiled=True)]
    reduce_scatter x2 -> x0, waiting for transfers between devices: 36.8 us -> none  [the longest x1 18.6 us: shards(): lax.psum_scatter(partial_sum.astype(jnp.bfloat16), 'tp', scatter_dimensio...]
    all_gather x1 -> x0, waiting for transfers between devices: 22.8 us -> none  [shards(): gathered = lax.all_gather(totals[None], 'ep', axis=0, tiled=True)]
    all_to_all x1 -> x0, starting transfers between devices: 5.23 us -> none  [shards(): lax.all_to_all(summed, 'ep', split_axis=0, concat_axis=0, tiled=True)]
    unnamed x15 -> x14, local copies, waits for them, and re-layouts: 3.23 us -> 5.74 us
    dot_general x1, matrix products: 2.35 us -> 4.66 us  [expert_hidden(): jnp.dot(flattened, gate_shard, preferred_element_type=jnp.float32)]
  transfers between devices with their start and end apart: 4 -> 0, of which waited for: 3 -> 0; matrix products, arithmetic and copies ran while one was open for 2% -> 0% of each run, Pallas kernels for 9% -> 0%
where the time goes in v1:
time: 102 us; the launch traced here: 101 us
  Pallas kernels  75.5 us (74%)
  matrix products  14.9 us (15%)
  local copies, waits for them, and re-layouts  6.43 us (6%)
  other arithmetic  3.59 us (4%)
    pallas_call x1, Pallas kernels, return_pass(): pl.pallas_call(functools.partial(return_kernel, ep_count, tp_count), out_...  31.7 us
    pallas_call x1, Pallas kernels, dispatch_pass(): pl.pallas_call(functools.partial(dispatch_kernel, ep_count, tp_count), ou...  28.8 us
    pallas_call x1, Pallas kernels, local_pass(): pl.pallas_call(functools.partial(local_kernel, heads, width), out_shape=(...  10.2 us
    unnamed x14, local copies, waits for them, and re-layouts  5.74 us
    pallas_call x1, Pallas kernels, finish_pass(): pl.pallas_call(functools.partial(finish_kernel, heads, width), out_shape=...  4.76 us
    dot_general x1, matrix products, expert_hidden(): jnp.dot(flattened, gate_shard, preferred_element_type=jnp.float32)  4.66 us
    dot_general x1, matrix products, shards(): jnp.dot(hidden.reshape(-1, hidden.shape[-1]), down_shard, preferred_eleme...  3.72 us
    dot_general x1, matrix products, expert_hidden(): up_part = jnp.dot(flattened, up_shard, preferred_element_type=jnp.float32)  2.54 us

profile of v1, /device:TPU:1, one launch (start us, length us, event | category | flops | bytes accessed | tf_op | source)
XLA Modules:
  0.0 101.2 jit_solution(8064448430756234259)
XLA Ops:
  0.6 0.7 convert_element_type.45
  1.3 1.2 %fusion.11 = f32[128]{0:T(128)S(1)} fusion(bf16[128,2048]{1,0:T(8,128)(2,1)} %param.33), kind=kLoop, calls=%fused_computation.12 | loop fusion | flops 786304 | bytes 524800 | tf_op jit(solution)/shard_map/reduce_sum | solution.py:17
  2.6 0.8 copy.40
  3.3 0.1 eq.42
  3.5 0.1 eq.38
  3.6 0.6 reduce-window.6
  4.2 0.2 slice_reduce_fusion
  4.5 0.1 fusion.21
  4.6 0.1 reduce_sum.42
  4.7 0.1 copy.42
  4.8 0.7 multiply_add_fusion
  5.5 1.4 %copy.44.shift_ref = f32[128,4]{1,0:T(8,128)} copy(f32[128,4]{0,1:T(4,128)} %param.30) | data formatting | bytes 4096 | tf_op args[10]
  6.9 0.1 fusion.18
  7.0 0.1 convert_reduce_fusion
  7.2 2.0 %copy.43.low_ref = bf16[2048,64]{1,0:T(8,128)(2,1)} copy(bf16[2048,64]{0,1:T(8,128)(2,1)} %param.25) | data formatting | bytes 524288 | tf_op args[5]
  9.1 0.0 copy-start
  9.1 0.0 copy-start.1
  9.1 10.2 %mix_local.1 = (bf16[2,4,64,128]{3,2,1,0:T(8,128)(2,1)}, bf16[128,512]{1,0:T(8,128)(2,1)}, f32[128,256]{1,0:T(8,128)}) custom-call(bf16[128,2048]{1,0:T(8,128)(2,1)} %rows_ref.1, f32[1,2048]{1,0:T(1,128)} %bitcast.40, bf16[2048,256]{1,0:T(8,128)(2,1)} %recept_ref.1, bf16[2048,256]{1,0:T(8,128)(2,1)} %key_ref.1, bf16[2048,256]{1,0:T(8,128)(2,1)} %value_ref.1, ...), custom_call_target="tpu_custom_call" | custom-call | flops 2000000000 | bytes 20000000 | tf_op jit(solution)/shard_map/mix_local/pallas_call | solution.py:217
  19.3 0.0 copy-done
  19.3 0.0 copy-done.1
  19.3 2.1 %convolution_convert_fusion = bf16[512,2048]{1,0:T(8,128)(2,1)} fusion(bf16[128,2048]{1,0:T(8,128)(2,1)S(1)} %copy-done, f32[2048]{0:T(1024)S(1)} %copy-done.1, f32[128]{0:T(128)S(1)} %add_rsqrt_fusion, s32[128,512]{1,0:T(8,128)S(1)} %convert_reduce_fusion), kind=kOutput, calls=%fused_computation.7 | convolution fusion | flops 270598144 | bytes 2892288 | tf_op jit(solution)/shard_map/dot_general | solution.py:594
  21.4 28.8 %dispatch.1 = (bf16[8,64,2048]{2,1,0:T(8,128)(2,1)}, bf16[8,4,64,128]{3,2,1,0:T(8,128)(2,1)}) custom-call(bf16[8,64,2048]{2,1,0:T(8,128)(2,1)} %bitcast.36, bf16[2,4,64,128]{3,2,1,0:T(8,128)(2,1)} %get-tuple-element.9.totals_ref), custom_call_target="tpu_custom_call" | custom-call | tf_op jit(solution)/shard_map/dispatch/pallas_call | solution.py:365
  50.2 0.0 copy-start.4
  50.3 4.8 %mix_finish.1.mix_ref = bf16[128,2048]{1,0:T(8,128)(2,1)} custom-call(s32[1]{0:T(128)} %bitcast.12.where_ref, bf16[8,4,64,128]{3,2,1,0:T(8,128)(2,1)} %get-tuple-element.11.totals_ref, bf16[128,512]{1,0:T(8,128)(2,1)} %get-tuple-element.12.read_ref, f32[128,256]{1,0:T(8,128)} %get-tuple-element.13.own_ref, f32[1,256]{1,0:T(1,128)} %bitcast.43, ...), custom_call_target="tpu_custom_call" | custom-call | flops 1000000000 | bytes 10000000 | tf_op jit(solution)/shard_map/mix_finish/pallas_call | solution.py:234
  55.0 0.0 copy-done.4
  55.0 0.0 copy-start.2
  55.0 4.7 %fusion.4 = f32[512,1024]{1,0:T(8,128)S(1)} fusion(bf16[512,2048]{1,0:T(8,128)(2,1)S(1)} %bitcast.38, bf16[1,2048,1024]{2,1,0:T(8,128)(2,1)} %param.37), kind=kOutput, calls=%fused_computation.4 | convolution fusion | flops 2147483648 | bytes 8388608 | tf_op jit(solution)/shard_map/dot_general | solution.py:544
  59.7 0.0 copy-done.2
  59.7 0.0 copy-start.3
  59.7 2.5 %multiply_convert_fusion = bf16[512,1024]{1,0:T(8,128)(2,1)S(1)} fusion(f32[512,1024]{1,0:T(8,128)S(1)} %fusion.4, bf16[512,2048]{1,0:T(8,128)(2,1)S(1)} %bitcast.39, bf16[1,2048,1024]{2,1,0:T(8,128)(2,1)S(1)} %copy-done.2), kind=kOutput, calls=%fused_computation.8 | convolution fusion | flops 2150629376 | bytes 9437184 | tf_op jit(solution)/shard_map/dot_general | solution.py:545
  62.3 0.0 copy-done.3
  62.3 3.7 %fusion.6.partial_ref = bf16[8,64,2048]{2,1,0:T(8,128)(2,1)} fusion(bf16[8,64,1024]{2,1,0:T(8,128)(2,1)S(1)} %bitcast.44, bf16[1,1024,2048]{2,1,0:T(8,128)(2,1)S(1)} %copy-done.3), kind=kOutput, calls=%fused_computation.6 | convolution fusion | flops 2148532224 | bytes 7340032 | tf_op jit(solution)/shard_map/dot_general | solution.py:615
  66.0 31.7 %return.1 = (bf16[8,64,512]{2,1,0:T(8,128)(2,1)}, bf16[32,2048]{1,0:T(8,128)(2,1)}) custom-call(bf16[8,64,2048]{2,1,0:T(8,128)(2,1)} %fusion.6.partial_ref, bf16[128,2048]{1,0:T(8,128)(2,1)} %mix_finish.1.mix_ref), custom_call_target="tpu_custom_call" | custom-call | tf_op jit(solution)/shard_map/return/pallas_call | solution.py:499
  97.7 1.9 %convolution_convert_fusion.1 = bf16[128,512]{1,0:T(8,128)(2,1)} fusion(bf16[128,512]{1,0:T(8,128)(2,1)S(1)} %fusion.18, bf16[512,512]{1,0:T(8,128)(2,1)} %bitcast.37), kind=kOutput, calls=%fused_computation.11 | convolution fusion | flops 67174400 | bytes 786432 | tf_op jit(solution)/shard_map/dot_general | solution.py:625
  99.7 1.6 %copy.46 = bf16[32,2048]{1,0:T(8,128)(2,1)} copy(bf16[32,2048]{1,0:T(8,128)(2,1)} %get-tuple-element.18) | data formatting | bytes 262144
  (4 shorter events, 0.1 us)
Async XLA Ops:
  9.1 10.2 %copy-start = (bf16[128,2048]{1,0:T(8,128)(2,1)S(1)}, bf16[128,2048]{1,0:T(8,128)(2,1)}, u32[]{:S(2)}) copy-start(bf16[128,2048]{1,0:T(8,128)(2,1)} %param.33) | copy-start | bytes 1572868
  9.1 10.2 %copy-start.1 = (f32[2048]{0:T(1024)S(1)}, f32[2048]{0:T(1024)}, u32[]{:S(2)}) copy-start(f32[2048]{0:T(1024)} %param.34) | copy-start | bytes 24580
  50.2 4.8 %copy-start.4 = (bf16[8,64,2048]{2,1,0:T(8,128)(2,1)S(1)}, bf16[8,64,2048]{2,1,0:T(8,128)(2,1)}, u32[]{:S(2)}) copy-start(bf16[8,64,2048]{2,1,0:T(8,128)(2,1)} %get-tuple-element.10) | copy-start | bytes 6291460
  55.0 4.7 %copy-start.2 = (bf16[1,2048,1024]{2,1,0:T(8,128)(2,1)S(1)}, bf16[1,2048,1024]{2,1,0:T(8,128)(2,1)}, u32[]{:S(2)}) copy-start(bf16[1,2048,1024]{2,1,0:T(8,128)(2,1)} %param.38) | copy-start | bytes 12582916
  59.7 2.6 %copy-start.3 = (bf16[1,1024,2048]{2,1,0:T(8,128)(2,1)S(1)}, bf16[1,1024,2048]{2,1,0:T(8,128)(2,1)}, u32[]{:S(2)}) copy-start(bf16[1,1024,2048]{2,1,0:T(8,128)(2,1)} %param.39) | copy-start | bytes 12582916

commit v2 on v1

--- a/solution.py
+++ b/solution.py
@@ -49,6 +49,7 @@
     totals_ref,
     read_ref,
     own_ref,
+    midway=None,
 ):
     tokens = rows_ref.shape[0]
     chunk = min(CHUNK, tokens)
@@ -142,6 +143,8 @@
         for p in problems:
             inverses[p] = inverses[p] - mul(inverses[p], right[p])
         size = 2 * size
+    if midway is not None:
+        midway()
     eye = lax.broadcasted_iota(jnp.int32, (width, width), 0) == lax.broadcasted_iota(
         jnp.int32, (width, width), 1
     )
@@ -185,8 +188,11 @@
         own_ref[:, cut] = own_sum
 
 
-def finish_kernel(heads, width, where_ref, totals_ref, read_ref, own_ref, gain_ref, out_ref, res):
-    me = where_ref[0]
+def finish_kernel(heads, width, where_ref, *refs):
+    finish_body(heads, width, where_ref[0], *refs)
+
+
+def finish_body(heads, width, me, totals_ref, read_ref, own_ref, gain_ref, out_ref, res):
     count = totals_ref.shape[0]
     states = {(d, h): jnp.zeros((width, width), F32) for d in range(2) for h in range(heads)}
     for j in range(count):
@@ -273,12 +279,27 @@
 
 
 def dispatch_kernel(
+    heads,
+    head_width,
     ep_count,
     tp_count,
     buffer_ref,
-    totals_ref,
+    rows_ref,
+    gain_ref,
+    recept_ref,
+    key_ref,
+    value_ref,
+    low_ref,
+    decay_up_ref,
+    rate_up_ref,
+    decay_base_ref,
+    rate_base_ref,
+    shift_ref,
     arrived_ref,
     gathered_ref,
+    read_ref,
+    own_ref,
+    totals_ref,
     ep_send,
     ep_recv,
     row_send,
@@ -310,23 +331,10 @@
         )
         copy.start()
         first.append(copy)
-    for k in range(1, ep_count):
-        peer = lax.rem(me + k, ep_count)
-        direction = jnp.where(peer > me, 0, 1)
-        copy = remote(
-            totals_ref.at[direction],
-            gathered_ref.at[me],
-            total_send.at[k],
-            total_recv.at[k],
-            (peer, lane),
-        )
-        copy.start()
-        sums.append(copy)
     keep = pltpu.make_async_copy(buffer_ref.at[me], arrived_ref.at[me], keep_sem.at[0])
     keep.start()
-    keep_total = pltpu.make_async_copy(totals_ref.at[0], gathered_ref.at[me], keep_sem.at[1])
-    keep_total.start()
-    for k in range(1, ep_count):
+
+    def forward(k):
         owner = lax.rem(me + ep_count - k, ep_count)
         first[k - 1].wait_recv()
         block = arrived_ref.at[owner, :, columns(lane)]
@@ -343,6 +351,48 @@
         copy = remote(block, block, pair_send.at[0, k], pair_recv.at[0, k], (me, mate))
         copy.start()
         third.append(copy)
+
+    early = ep_count // 2
+
+    def midway():
+        for k in range(1, early):
+            forward(k)
+
+    local_kernel(
+        heads,
+        head_width,
+        rows_ref,
+        gain_ref,
+        recept_ref,
+        key_ref,
+        value_ref,
+        low_ref,
+        decay_up_ref,
+        rate_up_ref,
+        decay_base_ref,
+        rate_base_ref,
+        shift_ref,
+        totals_ref,
+        read_ref,
+        own_ref,
+        midway,
+    )
+    for k in range(1, ep_count):
+        peer = lax.rem(me + k, ep_count)
+        direction = jnp.where(peer > me, 0, 1)
+        copy = remote(
+            totals_ref.at[direction],
+            gathered_ref.at[me],
+            total_send.at[k],
+            total_recv.at[k],
+            (peer, lane),
+        )
+        copy.start()
+        sums.append(copy)
+    keep_total = pltpu.make_async_copy(totals_ref.at[0], gathered_ref.at[me], keep_sem.at[1])
+    keep_total.start()
+    for k in range(early, ep_count):
+        forward(k)
     for j, owner, k, copy in second:
         copy.wait_recv()
         block = arrived_ref.at[owner, :, columns(lax.rem(lane + tp_count - 2 * j, tp_count))]
@@ -359,18 +409,22 @@
     keep_total.wait()
 
 
-def dispatch_pass(ep_count, tp_count, buffer, totals):
+def dispatch_pass(heads, head_width, ep_count, tp_count, buffer, *operands):
+    tokens = operands[0].shape[0]
     rows = tp_count // 2
     dma = pltpu.SemaphoreType.DMA
     return pl.pallas_call(
-        functools.partial(dispatch_kernel, ep_count, tp_count),
+        functools.partial(dispatch_kernel, heads, head_width, ep_count, tp_count),
         out_shape=(
             jax.ShapeDtypeStruct(buffer.shape, BF16),
-            jax.ShapeDtypeStruct((ep_count,) + totals.shape[1:], BF16),
+            jax.ShapeDtypeStruct((ep_count, heads, head_width, 2 * head_width), BF16),
+            jax.ShapeDtypeStruct((tokens, 2 * heads * head_width), BF16),
+            jax.ShapeDtypeStruct((tokens, heads * head_width), F32),
         ),
-        in_specs=[pl.BlockSpec(memory_space=pltpu.VMEM)] * 2,
-        out_specs=(pl.BlockSpec(memory_space=pltpu.VMEM),) * 2,
+        in_specs=[pl.BlockSpec(memory_space=pltpu.VMEM)] * (1 + len(operands)),
+        out_specs=(pl.BlockSpec(memory_space=pltpu.VMEM),) * 4,
         scratch_shapes=[
+            pltpu.VMEM((2, heads, head_width, 2 * head_width), BF16),
             dma((ep_count,)),
             dma((ep_count,)),
             dma((rows, ep_count)),
@@ -383,16 +437,23 @@
         ],
         compiler_params=pltpu.CompilerParams(collective_id=1, has_side_effects=True),
         name="dispatch",
-    )(buffer, totals)
+    )(buffer, *operands)
 
 
 def return_kernel(
+    heads,
+    head_width,
     ep_count,
     tp_count,
     partial_ref,
-    mix_ref,
+    gathered_ref,
+    read_ref,
+    own_ref,
+    gain_ref,
+    out_ref,
     back_ref,
     mix_out_ref,
+    mix_ref,
     pair_in,
     pair_sum,
     row_in,
@@ -452,6 +513,9 @@
                 )
                 copy.start()
                 second.append(copy)
+    finish_body(
+        heads, head_width, me, gathered_ref, read_ref, own_ref, gain_ref, out_ref, mix_ref
+    )
     mixes = []
     for j in range(1, tp_count):
         peer = lax.rem(lane + j, tp_count)
@@ -490,21 +554,23 @@
         copy.wait_send()
 
 
-def return_pass(ep_count, tp_count, partial_sum, partial_mix):
+def return_pass(heads, head_width, ep_count, tp_count, partial_sum, *operands):
     rows = tp_count // 2
     dma = pltpu.SemaphoreType.DMA
     slots, features = partial_sum.shape[1:]
     width = features // tp_count
-    mix_rows = partial_mix.shape[0] // tp_count
+    tokens = operands[1].shape[0]
+    mix_rows = tokens // tp_count
     return pl.pallas_call(
-        functools.partial(return_kernel, ep_count, tp_count),
+        functools.partial(return_kernel, heads, head_width, ep_count, tp_count),
         out_shape=(
             jax.ShapeDtypeStruct((ep_count, slots, width), BF16),
             jax.ShapeDtypeStruct((mix_rows, features), BF16),
         ),
-        in_specs=[pl.BlockSpec(memory_space=pltpu.VMEM)] * 2,
+        in_specs=[pl.BlockSpec(memory_space=pltpu.VMEM)] * (1 + len(operands)),
         out_specs=(pl.BlockSpec(memory_space=pltpu.VMEM),) * 2,
         scratch_shapes=[
+            pltpu.VMEM((tokens, features), BF16),
             pltpu.VMEM((ep_count, rows, slots, width), BF16),
             pltpu.VMEM((ep_count, rows, slots, width), BF16),
             pltpu.VMEM((ep_count, rows, slots, width), BF16),
@@ -521,7 +587,7 @@
         ],
         compiler_params=pltpu.CompilerParams(collective_id=2, has_side_effects=True),
         name="return",
-    )(partial_sum, partial_mix)
+    )(partial_sum, *operands)
 
 
 def route_tables(route_rows, weight_rows, expert_count, slot_count):
@@ -571,9 +637,7 @@
 ):
     head_count = decay_shift.shape[1]
     head_width = w_recept.shape[1] // head_count
-    totals, read, own = local_pass(
-        head_count,
-        head_width,
+    mix_operands = (
         mixer_input_rows,
         mix_gain[None],
         w_recept,
@@ -601,24 +665,28 @@
     lanes = lax.axis_size("tp")
     small = experts <= 8 and lanes == 4
     if small:
-        arrived, gathered = dispatch_pass(experts, lanes, buffer, totals)
+        arrived, gathered, read, own = dispatch_pass(
+            head_count, head_width, experts, lanes, buffer, *mix_operands
+        )
     else:
+        totals, read, own = local_pass(head_count, head_width, *mix_operands)
         arrived = lax.all_to_all(buffer, "ep", split_axis=0, concat_axis=0, tiled=True)
         both = lax.all_gather(totals[None], "ep", axis=0, tiled=True)
         owners = jnp.arange(experts)[:, None, None, None]
         gathered = jnp.where(owners < lax.axis_index("ep"), both[:, 0], both[:, 1])
-    where = lax.axis_index("ep").astype(jnp.int32)[None]
-    partial_mix = finish_pass(
-        head_count, head_width, where, gathered, read, own, out_gain[None], w_output
-    )
+    finish_operands = (gathered, read, own, out_gain[None], w_output)
     hidden = expert_hidden(arrived, gate_shard, up_shard)
     partial_sum = jnp.dot(
         hidden.reshape(-1, hidden.shape[-1]), down_shard, preferred_element_type=jnp.float32
     )
     partial_sum = partial_sum.reshape(experts, slots, -1).astype(jnp.bfloat16)
     if small:
-        returned, mix_out = return_pass(experts, lanes, partial_sum, partial_mix)
+        returned, mix_out = return_pass(
+            head_count, head_width, experts, lanes, partial_sum, *finish_operands
+        )
     else:
+        where = lax.axis_index("ep").astype(jnp.int32)[None]
+        partial_mix = finish_pass(head_count, head_width, where, *finish_operands)
         mix_out = lax.psum_scatter(partial_mix, "tp", scatter_dimension=0, tiled=True)
         summed = lax.psum_scatter(partial_sum, "tp", scatter_dimension=2, tiled=True)
         returned = lax.all_to_all(summed, "ep", split_axis=0, concat_axis=0, tiled=True)

time: 102 us -> 87.7 us (0.86)
  Pallas kernels: 75.5 us -> 62.2 us
  matrix products: 14.9 us -> 16.7 us
  local copies, waits for them, and re-layouts: 6.43 us -> 4.89 us
    pallas_call x4 -> x2, Pallas kernels: 75.5 us -> 62.2 us  [the longest x1 31.5 us: dispatch_pass(): pl.pallas_call(functools.partial(dispatch_kernel, heads, head_width, ep_c...]
    unnamed x14 -> x16, local copies, waits for them, and re-layouts: 5.74 us -> 4.2 us
    dot_general x1, matrix products: 2.1 us -> 3.21 us  [shards(): lax.dot_general(placing, moe_normed, (((0,), (0,)), ((), ())), preferred_...]
where the time goes in v2:
time: 87.7 us; the launch traced here: 87.5 us
  Pallas kernels  62.2 us (71%)
  matrix products  16.7 us (19%)
  local copies, waits for them, and re-layouts  4.89 us (6%)
  other arithmetic  2.92 us (3%)
    pallas_call x1, Pallas kernels, dispatch_pass(): pl.pallas_call(functools.partial(dispatch_kernel, heads, head_width, ep_c...  31.5 us
    pallas_call x1, Pallas kernels, return_pass(): pl.pallas_call(functools.partial(return_kernel, heads, head_width, ep_cou...  30.7 us
    dot_general x1, matrix products, expert_hidden(): jnp.dot(flattened, gate_shard, preferred_element_type=jnp.float32)  5.3 us
    unnamed x16, local copies, waits for them, and re-layouts  4.2 us
    dot_general x1, matrix products, shards(): jnp.dot(hidden.reshape(-1, hidden.shape[-1]), down_shard, preferred_eleme...  3.72 us
    dot_general x1, matrix products, shards(): lax.dot_general(placing, moe_normed, (((0,), (0,)), ((), ())), preferred_...  3.21 us
    dot_general x1, matrix products, expert_hidden(): up_part = jnp.dot(flattened, up_shard, preferred_element_type=jnp.float32)  2.51 us
    dot_general x1, matrix products, shards(): jnp.dot(weighing, returned.reshape(experts * slots, -1), preferred_elemen...  1.93 us

profile of v2, /device:TPU:1, one launch (start us, length us, event | category | flops | bytes accessed | tf_op | source)
XLA Modules:
  0.0 87.5 jit_solution(1142701018307849785)
XLA Ops:
  0.6 0.0 copy-start
  0.6 0.8 copy.40
  1.5 0.1 eq.42
  1.6 0.6 reduce-window.6
  2.2 0.2 slice_reduce_fusion
  2.5 0.1 eq.38
  2.6 0.1 fusion.21
  2.7 0.1 reduce_sum.42
  2.8 0.1 copy.42
  2.9 0.7 multiply_add_fusion
  3.6 0.1 convert_reduce_fusion
  3.7 0.0 copy-start.1
  3.7 1.2 %fusion.11 = f32[128]{0:T(128)S(1)} fusion(bf16[128,2048]{1,0:T(8,128)(2,1)} %param.33), kind=kLoop, calls=%fused_computation.12 | loop fusion | flops 786304 | bytes 524800 | tf_op jit(solution)/shard_map/reduce_sum | solution.py:17
  5.0 3.2 %convolution_convert_fusion = bf16[512,2048]{1,0:T(8,128)(2,1)} fusion(bf16[128,2048]{1,0:T(8,128)(2,1)} %param.33, f32[2048]{0:T(1024)} %param.34, f32[128]{0:T(128)S(1)} %add_rsqrt_fusion, s32[128,512]{1,0:T(8,128)S(1)} %convert_reduce_fusion), kind=kOutput, calls=%fused_computation.7 | convolution fusion | flops 270598144 | bytes 2892288 | tf_op jit(solution)/shard_map/dot_general | solution.py:658
  8.2 0.0 copy-done
  8.2 1.0 %copy.43.low_ref = bf16[2048,64]{1,0:T(8,128)(2,1)} copy(bf16[2048,64]{0,1:T(8,128)(2,1)S(1)} %copy-done) | data formatting | bytes 524288 | tf_op args[5]
  9.2 0.0 copy-done.1
  9.2 0.7 copy.44.shift_ref
  10.0 31.5 %dispatch.1 = (bf16[8,64,2048]{2,1,0:T(8,128)(2,1)}, bf16[8,4,64,128]{3,2,1,0:T(8,128)(2,1)}, bf16[128,512]{1,0:T(8,128)(2,1)}, f32[128,256]{1,0:T(8,128)}) custom-call(bf16[8,64,2048]{2,1,0:T(8,128)(2,1)} %bitcast.35, bf16[128,2048]{1,0:T(8,128)(2,1)} %rows_ref.1, f32[1,2048]{1,0:T(1,128)} %bitcast.37, bf16[2048,256]{1,0:T(8,128)(2,1)} %recept_ref.1, ...), custom_call_target="tpu_custom_call" | custom-call | tf_op jit(solution)/shard_map/dispatch/pallas_call | solution.py:416
  41.5 0.0 copy-start.2
  41.5 0.0 copy-start.4
  41.5 5.3 %fusion.4 = f32[512,1024]{1,0:T(8,128)S(1)} fusion(bf16[512,2048]{1,0:T(8,128)(2,1)} %bitcast.41, bf16[1,2048,1024]{2,1,0:T(8,128)(2,1)} %param.37), kind=kOutput, calls=%fused_computation.4 | convolution fusion | flops 2147483648 | bytes 8388608 | tf_op jit(solution)/shard_map/dot_general | solution.py:610
  46.8 0.0 copy-done.2
  46.8 0.0 copy-done.4
  46.8 0.0 copy-start.3
  46.9 2.5 %multiply_convert_fusion = bf16[512,1024]{1,0:T(8,128)(2,1)S(1)} fusion(f32[512,1024]{1,0:T(8,128)S(1)} %fusion.4, bf16[512,2048]{1,0:T(8,128)(2,1)S(1)} %bitcast.42, bf16[1,2048,1024]{2,1,0:T(8,128)(2,1)S(1)} %copy-done.2), kind=kOutput, calls=%fused_computation.8 | convolution fusion | flops 2150629376 | bytes 9437184 | tf_op jit(solution)/shard_map/dot_general | solution.py:611
  49.4 0.0 copy-done.3
  49.4 3.7 %fusion.6.partial_ref = bf16[8,64,2048]{2,1,0:T(8,128)(2,1)} fusion(bf16[8,64,1024]{2,1,0:T(8,128)(2,1)S(1)} %bitcast.43, bf16[1,1024,2048]{2,1,0:T(8,128)(2,1)S(1)} %copy-done.3), kind=kOutput, calls=%fused_computation.6 | convolution fusion | flops 2148532224 | bytes 7340032 | tf_op jit(solution)/shard_map/dot_general | solution.py:679
  53.1 0.0 copy-start.5
  53.1 30.7 %return.1 = (bf16[8,64,512]{2,1,0:T(8,128)(2,1)}, bf16[32,2048]{1,0:T(8,128)(2,1)}) custom-call(bf16[8,64,2048]{2,1,0:T(8,128)(2,1)} %fusion.6.partial_ref, bf16[8,4,64,128]{3,2,1,0:T(8,128)(2,1)} %get-tuple-element.9.gathered_ref, bf16[128,512]{1,0:T(8,128)(2,1)} %get-tuple-element.10.read_ref, f32[128,256]{1,0:T(8,128)} %get-tuple-element.11.own_ref, ...), custom_call_target="tpu_custom_call" | custom-call | tf_op jit(solution)/shard_map/return/pallas_call | solution.py:564
  83.8 0.0 copy-done.5
  83.8 0.1 fusion.18
  84.0 1.9 %convolution_convert_fusion.1 = bf16[128,512]{1,0:T(8,128)(2,1)} fusion(bf16[128,512]{1,0:T(8,128)(2,1)S(1)} %fusion.18, bf16[512,512]{1,0:T(8,128)(2,1)} %bitcast.36), kind=kOutput, calls=%fused_computation.11 | convolution fusion | flops 67174400 | bytes 786432 | tf_op jit(solution)/shard_map/dot_general | solution.py:693
  85.9 1.6 %copy.46 = bf16[32,2048]{1,0:T(8,128)(2,1)} copy(bf16[32,2048]{1,0:T(8,128)(2,1)} %get-tuple-element.16) | data formatting | bytes 262144
  (5 shorter events, 0.1 us)
Async XLA Ops:
  0.6 7.6 %copy-start = (bf16[2048,64]{0,1:T(8,128)(2,1)S(1)}, bf16[2048,64]{0,1:T(8,128)(2,1)}, u32[]{:S(2)}) copy-start(bf16[2048,64]{0,1:T(8,128)(2,1)} %param.25) | copy-start | bytes 786436
  3.7 5.5 %copy-start.1 = (f32[128,4]{0,1:T(4,128)S(1)}, f32[128,4]{0,1:T(4,128)}, u32[]{:S(2)}) copy-start(f32[128,4]{0,1:T(4,128)} %param.30) | copy-start | bytes 6148
  41.5 5.3 %copy-start.2 = (bf16[1,2048,1024]{2,1,0:T(8,128)(2,1)S(1)}, bf16[1,2048,1024]{2,1,0:T(8,128)(2,1)}, u32[]{:S(2)}) copy-start(bf16[1,2048,1024]{2,1,0:T(8,128)(2,1)} %param.38) | copy-start | bytes 12582916
  41.5 5.3 %copy-start.4 = (bf16[8,64,2048]{2,1,0:T(8,128)(2,1)S(1)}, bf16[8,64,2048]{2,1,0:T(8,128)(2,1)}, u32[]{:S(2)}) copy-start(bf16[8,64,2048]{2,1,0:T(8,128)(2,1)} %get-tuple-element.8) | copy-start | bytes 6291460
  46.8 2.5 %copy-start.3 = (bf16[1,1024,2048]{2,1,0:T(8,128)(2,1)S(1)}, bf16[1,1024,2048]{2,1,0:T(8,128)(2,1)}, u32[]{:S(2)}) copy-start(bf16[1,1024,2048]{2,1,0:T(8,128)(2,1)} %param.39) | copy-start | bytes 12582916
  53.1 30.7 %copy-start.5 = (f32[128,2]{0,1:T(2,128)S(1)}, f32[128,2]{0,1:T(2,128)}, u32[]{:S(2)}) copy-start(f32[128,2]{0,1:T(2,128)} %param.36) | copy-start | bytes 3076
